TPU v7x, 32 devices: a whole 2x2x4 slice. The times are simulated.
32 devices in a mesh: fs: 8 (over z, y), tp: 4 (over x, core).
Axes of the slice: x: 2, y: 2, z: 4, core: 2. Of those that a mesh axis runs over, the one named last changes fastest.
Arguments:
- tokens: bfloat16 [8192, 2048], P('fs'), may hold values from -6 to 6
- norm_gain: float32 [2048], P('fs'), may hold values from 0.1 to 1.9
- gate_train: float32 [8, 2048, 768], P(None, 'fs', 'tp'), may hold values from -0.125 to 0.125
- up_train: float32 [8, 2048, 768], P(None, 'fs', 'tp'), may hold values from -0.125 to 0.125
- down_train: float32 [8, 768, 2048], P(None, 'fs', 'tp'), may hold values from -0.21875 to 0.21875
- expert_ids: int32 [8192, 2], P('fs'), may hold values from 0 to 7, all different within a row; in each aligned block of 1024 rows (0 to 1023, 1024 to 2047, ...) at most 512 rows name the same one
- route_weights: float32 [8192, 2], P('fs'), may hold values from 0.1 to 1
Outputs:
- gate_serve: bfloat16 [8, 2048, 768], P('fs', None, 'tp')
- up_serve: bfloat16 [8, 2048, 768], P('fs', None, 'tp')
- down_serve: bfloat16 [8, 768, 2048], P('fs', 'tp')
- mixed: bfloat16 [8192, 2048], P('fs', 'tp')
Inputs may be any that keep to these rules, and one draw needn't show every extreme that they name: `expert_ids`: each row names 2 different experts. Within each aligned block of 1024 rows no expert is named more than 512 times, and in every block some expert is named exactly 512 times; every expert is named somewhere.
All inputs are finite; a program needn't handle non-finite values.
Results may differ from a plain program's by a relative error of at most 0.011.
Values may be sent and summed in bfloat16 or wider, within the bound.
A program may use at most 128 MiB of HBM per device.

v0:
```python
import jax
import jax.numpy as jnp
from jax import lax
from jax.sharding import PartitionSpec as P

epsilon = 1e-06


def on_device(tokens, norm_gain, gate_train, up_train, down_train, expert_ids, route_weights):
    experts, rows, cols = gate_train.shape
    fs_at = lax.axis_index("fs")
    tok_rows, picks = expert_ids.shape
    down_rows, down_cols = down_train.shape[1:]
    fs_count = lax.axis_size("fs")
    gate_up = jnp.concatenate(
        [norm_gain[None, :, None] * gate_train, norm_gain[None, :, None] * up_train], axis=2
    ).astype(jnp.bfloat16)
    gate_up = gate_up.transpose(1, 0, 2).reshape(rows, experts * 2 * cols)
    gate_up_all = lax.all_gather(gate_up, "fs", axis=0, tiled=True)
    down_all = lax.all_gather(
        down_train.astype(jnp.bfloat16).reshape(experts * down_rows, down_cols),
        "fs",
        axis=0,
        tiled=True,
    )
    tok_float = tokens.astype(jnp.float32)
    normed = (
        tok_float * lax.rsqrt(jnp.mean(tok_float * tok_float, axis=-1, keepdims=True) + epsilon)
    ).astype(jnp.bfloat16)
    shares = route_weights / jnp.sum(route_weights, axis=-1, keepdims=True)
    group = 2 * lax.axis_size("tp")
    picked = [jnp.zeros((tok_rows, cols), jnp.float32) for _ in range(picks)]
    for first in range(0, experts, group):
        part = gate_up_all[:, first * 2 * cols : (first + group) * 2 * cols]
        if first:
            part, picked = lax.optimization_barrier((part, picked))
        acts = jnp.dot(normed, part, preferred_element_type=jnp.float32)
        for at in range(group):
            g = acts[:, at * 2 * cols : at * 2 * cols + cols]
            u = acts[:, at * 2 * cols + cols : (at + 1) * 2 * cols]
            h = jax.nn.silu(g) * u
            for k in range(picks):
                picked[k] = picked[k] + jnp.where(expert_ids[:, k : k + 1] == first + at, h, 0.0)
    hidden = jnp.stack([picked[k] * shares[:, k : k + 1] for k in range(picks)], 0)
    hidden_all = lax.all_gather(hidden.astype(jnp.bfloat16), "tp", axis=2, tiled=True)
    hidden_all = hidden_all.reshape(picks, tok_rows, fs_count, 1, down_rows)
    ids = jnp.arange(experts, dtype=jnp.int32)[None, None, :, None]
    mixed = jnp.zeros((tok_rows, down_cols), jnp.float32)
    for first in range(0, fs_count, group):
        blocks = hidden_all[:, :, first : first + group]
        if first:
            blocks, mixed = lax.optimization_barrier((blocks, mixed))
        spread = jnp.zeros((tok_rows, group, experts, down_rows), jnp.bfloat16)
        for k in range(picks):
            spread = jnp.where(expert_ids[:, k][:, None, None, None] == ids, blocks[k], spread)
        depth = experts * down_rows
        mixed = mixed + jnp.dot(
            spread.reshape(tok_rows, group * depth),
            down_all[first * depth : (first + group) * depth],
            preferred_element_type=jnp.float32,
        )
    mixed = mixed.astype(jnp.bfloat16)
    own = lax.dynamic_slice_in_dim(gate_up_all, fs_at * 2 * cols, 2 * cols, 1)
    down_own = lax.dynamic_slice_in_dim(
        down_all.reshape(fs_count, experts, down_rows, down_cols), fs_at, 1, 1
    ).reshape(1, fs_count * down_rows, down_cols)
    down_serve = lax.all_to_all(down_own, "tp", split_axis=1, concat_axis=2, tiled=True)
    return (own[None, :, :cols], own[None, :, cols:], down_serve, mixed)


def solution(mesh):
    return jax.shard_map(
        on_device,
        mesh=mesh,
        in_specs=(
            P("fs", None),
            P("fs"),
            P(None, "fs", "tp"),
            P(None, "fs", "tp"),
            P(None, "fs", "tp"),
            P("fs", None),
            P("fs", None),
        ),
        out_specs=(P("fs", None, "tp"), P("fs", None, "tp"), P("fs", "tp", None), P("fs", "tp")),
        check_vma=False,
    )
```

profile of v0, /device:TPU:0, one launch (start us, length us, event | category | flops | bytes accessed | tf_op | source)
XLA Modules:
  0.0 353.5 jit_solution(751838854216082823)
XLA Ops:
  7.2 0.0 all-gather.4.cloned.1.call-start
  7.2 2.3 multiply_convert_fusion.1
  9.6 1.3 pad_maximum_fusion
  10.9 0.0 all-gather.6.cloned.1.call-start
  10.9 1.0 convert_element_type.14
  11.9 0.0 all-gather.8.cloned.1.call-start
  12.0 0.2 compare_reduce_fusion.15
  12.2 3.1 fusion
  15.4 174.5 %all-gather.4.cloned.1.call-done = bf16[2048,3072]{0,1:T(8,128)(2,1)} async-done(((bf16[256,3072]{0,1:T(8,128)(2,1)}), bf16[2048,3072]{0,1:T(8,128)(2,1)}) %all-gather.4.cloned.1.call-update) | async-done | bytes 12582928 | tf_op jit(solution)/shard_map/all_gather | solution.py:19
  189.9 17.1 %fusion.2 = f32[1024,3072]{1,0:T(8,128)S(1)} fusion(bf16[2048,3072]{0,1:T(8,128)(2,1)} %all-gather.4.cloned.1.call-done, bf16[1024,2048]{1,0:T(8,128)(2,1)} %param.7, f32[1024]{0:T(1024)S(1)} %add_rsqrt_fusion), kind=kOutput, calls=%fused_computation.5 | convolution fusion | flops 12891193344 | bytes 29364224 | tf_op jit(solution)/shard_map/dot_general | solution.py:37
  207.0 4.5 %fusion.5 = bf16[1,1024,192]{2,1,0:T(8,128)(2,1)S(1)} fusion(f32[1024]{0:T(1024)S(1)} %bitcast.47, pred[1024]{0:T(1024)(128)(4,1)S(1)} %get-tuple-element.19, pred[1024]{0:T(1024)(128)(4,1)S(1)} %get-tuple-element.18, pred[1024]{0:T(1024)(128)(4,1)S(1)} %get-tuple-element.17, pred[1024]{0:T(1024)(128)(4,1)S(1)} %get-tuple-element.16, ...), kind=kLoop, calls=%fused_computation.24 | loop fusion | flops 11206656 | bytes 12988416 | tf_op jit(solution)/shard_map/stack | solution.py:44
  211.5 4.5 %fusion.6 = bf16[1,1024,192]{2,1,0:T(8,128)(2,1)S(1)} fusion(f32[1024]{0:T(1024)S(1)} %bitcast.46, pred[1024]{0:T(1024)(128)(4,1)S(1)} %get-tuple-element.12, pred[1024]{0:T(1024)(128)(4,1)S(1)} %get-tuple-element.11, pred[1024]{0:T(1024)(128)(4,1)S(1)} %get-tuple-element.10, pred[1024]{0:T(1024)(128)(4,1)S(1)} %get-tuple-element.9, ...), kind=kLoop, calls=%fused_computation.25 | loop fusion | flops 11206656 | bytes 12988416 | tf_op jit(solution)/shard_map/stack | solution.py:44
  216.0 0.2 pad_maximum_fusion.1
  216.2 2.0 copy.22
  218.2 71.3 %all-gather.6.cloned.1.call-done = bf16[6144,512]{1,0:T(8,128)(2,1)} async-done(((bf16[768,512]{1,0:T(8,128)(2,1)}), bf16[6144,512]{1,0:T(8,128)(2,1)}) %all-gather.6.cloned.1.call-update) | async-done | bytes 6291472 | tf_op jit(solution)/shard_map/all_gather | solution.py:20
  289.5 1.2 constant_dynamic-slice_fusion
  290.8 1.2 copy.30
  292.0 0.5 broadcast.126
  292.5 5.4 %reduce.32 = bf16[768,512]{1,0:T(8,128)(2,1)S(1)} reduce(bf16[768,1,512]{2,1,0:T(2,128)(2,1)S(1)} %bitcast.37, bf16[]{:T(256)} %broadcast.126), dimensions={1}, to_apply=%bitcast.32.reduce_sub_computation | reduce | bytes 1572866
  297.9 1.4 reshape.117
  299.3 3.7 %all-to-all-start = ((bf16[4,2,49152]{2,1,0:T(2,128)(2,1)}), bf16[4,2,49152]{2,1,0:T(2,128)(2,1)S(1)}, u32[]{:S(2)}, u32[]{:S(2)}) async-start(bf16[4,2,49152]{2,1,0:T(2,128)(2,1)} %reshape.117), calls=%async_computation | async-start | bytes 1572864 | tf_op jit(solution)/shard_map/all_to_all | solution.py:67
  303.0 20.2 %all-to-all-done = bf16[4,2,49152]{2,1,0:T(2,128)(2,1)S(1)} async-done(((bf16[4,2,49152]{2,1,0:T(2,128)(2,1)}), bf16[4,2,49152]{2,1,0:T(2,128)(2,1)S(1)}, u32[]{:S(2)}, u32[]{:S(2)}) %all-to-all-start) | async-done | bytes 786464 | tf_op jit(solution)/shard_map/all_to_all | solution.py:67
  323.2 0.7 reshape.118
  324.0 0.2 copy.25
  324.2 1.0 copy.28
  325.2 2.7 dynamic-slice_bitcast_fusion
  327.9 7.8 %fusion.7 = (bf16[1,1024,768]{1,0,2:T(2,128)(2,1)S(1)}, bf16[1,1024,768]{1,0,2:T(2,128)(2,1)S(1)}) fusion(bf16[2,1024,768]{1,0,2:T(2,128)(2,1)} %all-gather.8.cloned.1.call-done), kind=kLoop, calls=%fused_computation.47 | loop fusion | bytes 6291456 | tf_op jit(solution)/shard_map/slice | solution.py:55
  335.7 0.6 copy.26
  336.3 0.6 copy.27
  336.9 1.9 select_select_fusion
  338.8 0.5 slice-done.1
  339.3 7.6 %convolution_convert_fusion = bf16[1024,512]{1,0:T(8,128)(2,1)} fusion(bf16[1024,6144]{0,1:T(8,128)(2,1)S(1)} %bitcast.33, bf16[6144,512]{1,0:T(8,128)(2,1)S(1)} %bitcast.45), kind=kOutput, calls=%fused_computation.10 | convolution fusion | flops 6442975232 | bytes 19922944 | tf_op jit(solution)/shard_map/dot_general | solution.py:57
  (20 shorter events, 0.1 us)
Async XLA Ops:
  7.2 3.8 %copy-start = (f32[8,96,512]{2,1,0:T(8,128)S(1)}, f32[8,96,512]{2,1,0:T(8,128)}, u32[]{:S(2)}) copy-start(f32[8,96,512]{2,1,0:T(8,128)} %param.11) | copy-start | bytes 4718596
  7.2 182.7 %all-gather.4.cloned.1.call-start = ((), (), s32[]{:S(2)}) async-start(), calls=%async_computation.1 | async-start | bytes 14155776 | tf_op jit(solution)/shard_map/all_gather | solution.py:19
  9.6 2.4 copy-start.2
  9.6 2.5 copy-start.1
  10.9 278.7 %all-gather.6.cloned.1.call-start = ((), (), s32[]{:S(2)}) async-start(), calls=%async_computation.2 | async-start | bytes 7077888 | tf_op jit(solution)/shard_map/all_gather | solution.py:20
  11.9 315.9 %all-gather.8.cloned.1.call-start = ((), (), s32[]{:S(2)}) async-start(), calls=%async_computation.3 | async-start | bytes 3932160 | tf_op jit(solution)/shard_map/all_gather | solution.py:45
  299.3 23.9 %all-to-all-start = ((bf16[4,2,49152]{2,1,0:T(2,128)(2,1)}), bf16[4,2,49152]{2,1,0:T(2,128)(2,1)S(1)}, u32[]{:S(2)}, u32[]{:S(2)}) async-start(bf16[4,2,49152]{2,1,0:T(2,128)(2,1)} %reshape.117), calls=%async_computation | async-start | bytes 1572864 | tf_op jit(solution)/shard_map/all_to_all | solution.py:67
  336.3 2.5 slice-start
  336.9 2.4 slice-start.1
Sparse Core Ops, SparseCore 0:
  11.0 178.8 all-gather.3
  192.6 96.8 all-gather.5
  291.7 35.1 all-gather.7
where the time goes:
time: 354 us; the launch traced here: 353 us
  waiting for transfers between devices  266 us (75%)
  matrix products  24.7 us (7%)
  other arithmetic  24.4 us (7%)
  local copies, waits for them, and re-layouts  20.5 us (6%)
  between operations  14 us (4%)
  starting transfers between devices  3.8 us (1%)
    all_gather x1, waiting for transfers between devices, on_device(): gate_up_all = lax.all_gather(gate_up, 'fs', axis=0, tiled=True)  175 us
    all_gather x1, waiting for transfers between devices, on_device(): lax.all_gather(down_train.astype(jnp.bfloat16).reshape(experts * down_row...  71.3 us
    all_to_all x1, waiting for transfers between devices, on_device(): lax.all_to_all(down_own, 'tp', split_axis=1, concat_axis=2, tiled=True)  20.2 us
    dot_general x1, matrix products, on_device(): acts = jnp.dot(normed, part, preferred_element_type=jnp.float32)  17.1 us
    another operation x3, other arithmetic, on_device(): jnp.stack([picked[k] * shares[:, k:k + 1] for k in range(picks)], 0)  9.18 us
    slice x1, local copies, waits for them, and re-layouts, on_device(): blocks[k]  7.82 us
    dot_general x1, matrix products, on_device(): jnp.dot(spread.reshape(tok_rows, group * depth), down_all[first * depth:(...  7.64 us
  transfers between devices with their start and end apart: 4, of which 3 were waited for; matrix products, arithmetic and copies ran while one was open for 13% of the time, Pallas kernels for 0%

commit v1 on v0

--- a/solution.py
+++ b/solution.py
@@ -4,6 +4,27 @@
 from jax.sharding import PartitionSpec as P
 
 epsilon = 1e-06
+
+
+def ring_gather(x, axis, dim):
+    size, index, rows = (lax.axis_size(axis), lax.axis_index(axis), x.shape[dim])
+    right = [(i, (i + 1) % size) for i in range(size)]
+    behind = [(i, (i - 1) % size) for i in range(size)]
+    whole = jnp.zeros((*x.shape[:dim], size * rows, *x.shape[dim + 1 :]), x.dtype)
+    whole = lax.dynamic_update_slice_in_dim(whole, x, index * rows, axis=dim)
+    from_left = from_right = x
+    half = size // 2
+    for hop in range(1, half + 1):
+        from_left = lax.ppermute(from_left, axis, right)
+        whole = lax.dynamic_update_slice_in_dim(
+            whole, from_left, (index - hop) % size * rows, axis=dim
+        )
+        if hop < size - half:
+            from_right = lax.ppermute(from_right, axis, behind)
+            whole = lax.dynamic_update_slice_in_dim(
+                whole, from_right, (index + hop) % size * rows, axis=dim
+            )
+    return whole
 
 
 def on_device(tokens, norm_gain, gate_train, up_train, down_train, expert_ids, route_weights):
@@ -16,7 +37,7 @@
         [norm_gain[None, :, None] * gate_train, norm_gain[None, :, None] * up_train], axis=2
     ).astype(jnp.bfloat16)
     gate_up = gate_up.transpose(1, 0, 2).reshape(rows, experts * 2 * cols)
-    gate_up_all = lax.all_gather(gate_up, "fs", axis=0, tiled=True)
+    gate_up_all = ring_gather(gate_up, "fs", 0)
     down_all = lax.all_gather(
         down_train.astype(jnp.bfloat16).reshape(experts * down_rows, down_cols),
         "fs",

time: 354 us -> 453 us (1.28)
  waiting for transfers between devices: 266 us -> 319 us
  local copies, waits for them, and re-layouts: 20.5 us -> 45.2 us
  starting transfers between devices: 3.8 us -> 25.6 us
    ppermute x0 -> x7, waiting for transfers between devices: none -> 203 us  [the longest x4 203 us: ring_gather(): from_left = lax.ppermute(from_left, axis, right)]
    all_gather x1 -> x0, waiting for transfers between devices: 175 us -> none  [on_device(): gate_up_all = lax.all_gather(gate_up, 'fs', axis=0, tiled=True)]
    all_gather x1, waiting for transfers between devices: 0.01 us -> 23.1 us  [on_device(): lax.all_gather(hidden.astype(jnp.bfloat16), 'tp', axis=2, tiled=True)]
    all_gather x1, waiting for transfers between devices: 71.3 us -> 92.5 us  [on_device(): lax.all_gather(down_train.astype(jnp.bfloat16).reshape(experts * down_row...]
    ppermute x0 -> x7, starting transfers between devices: none -> 21 us  [the longest x4 10.6 us: ring_gather(): from_left = lax.ppermute(from_left, axis, right)]
    all_to_all x1, waiting for transfers between devices: 20.2 us -> 0.01 us  [on_device(): lax.all_to_all(down_own, 'tp', split_axis=1, concat_axis=2, tiled=True)]
    dynamic_update_slice x0 -> x8, local copies, waits for them, and re-layouts: none -> 15.2 us  [the longest x4 8.18 us: ring_gather(): lax.dynamic_update_slice_in_dim(whole, from_left, (index - hop) % size *...]
    broadcast_in_dim x0 -> x1, local copies, waits for them, and re-layouts: none -> 6.18 us  [ring_gather(): jnp.zeros((*x.shape[:dim], size * rows, *x.shape[dim + 1:]), x.dtype)]
  transfers between devices with their start and end apart: 4 -> 10, of which waited for: 3 -> 6; matrix products, arithmetic and copies ran while one was open for 13% -> 10% of each run, Pallas kernels for 0% -> 0%
where the time goes in v1:
time: 453 us
  waiting for transfers between devices  319 us (70%)
  local copies, waits for them, and re-layouts  45.2 us (10%)
  matrix products  25.7 us (6%)
  starting transfers between devices  25.6 us (6%)
  other arithmetic  23 us (5%)
  between operations  14.4 us (3%)
    ppermute x4, waiting for transfers between devices, ring_gather(): from_left = lax.ppermute(from_left, axis, right)  203 us
    all_gather x1, waiting for transfers between devices, on_device(): lax.all_gather(down_train.astype(jnp.bfloat16).reshape(experts * down_row...  92.5 us
    all_gather x1, waiting for transfers between devices, on_device(): lax.all_gather(hidden.astype(jnp.bfloat16), 'tp', axis=2, tiled=True)  23.1 us
    dot_general x1, matrix products, on_device(): acts = jnp.dot(normed, part, preferred_element_type=jnp.float32)  15.8 us
    ppermute x4, starting transfers between devices, ring_gather(): from_left = lax.ppermute(from_left, axis, right)  10.6 us
    ppermute x3, starting transfers between devices, ring_gather(): from_right = lax.ppermute(from_right, axis, behind)  10.4 us
    dot_general x1, matrix products, on_device(): jnp.dot(spread.reshape(tok_rows, group * depth), down_all[first * depth:(...  9.89 us
    another operation x3, other arithmetic, on_device(): jnp.stack([picked[k] * shares[:, k:k + 1] for k in range(picks)], 0)  9.2 us
  transfers between devices with their start and end apart: 10, of which 6 were waited for; matrix products, arithmetic and copies ran while one was open for 10% of the time, Pallas kernels for 0%

profile of v1, /device:TPU:0, one launch (start us, length us, event | category | flops | bytes accessed | tf_op | source)
XLA Modules:
  0.0 452.7 jit_solution(14677355470906214042)
XLA Ops:
  7.2 2.4 multiply_convert_fusion.1
  9.8 3.0 collective-permute-start
  12.8 3.1 collective-permute-start.1
  15.9 64.3 %collective-permute-done = bf16[256,3072]{0,1:T(8,128)(2,1)S(1)} collective-permute-done((bf16[256,3072]{0,1:T(8,128)(2,1)S(1)}, bf16[256,3072]{0,1:T(8,128)(2,1)S(1)}, u32[]{:S(2)}, u32[]{:S(2)}) %collective-permute-start) | collective-permute-done | bytes 1572896 | tf_op jit(solution)/shard_map/ppermute | solution.py:18
  80.2 2.5 collective-permute-start.2
  82.6 4.2 collective-permute-start.3
  86.9 62.3 %collective-permute-done.2 = bf16[256,3072]{0,1:T(8,128)(2,1)} collective-permute-done((bf16[256,3072]{0,1:T(8,128)(2,1)S(1)}, bf16[256,3072]{0,1:T(8,128)(2,1)}, u32[]{:S(2)}, u32[]{:S(2)}) %collective-permute-start.2) | collective-permute-done | bytes 1572896 | tf_op jit(solution)/shard_map/ppermute | solution.py:18
  149.1 2.6 collective-permute-start.4
  153.0 6.2 %broadcast_in_dim.181 = bf16[2048,3072]{0,1:T(8,128)(2,1)} broadcast(bf16[]{:T(256)} %constant.75.clone.1), dimensions={} | broadcast | bytes 12582914 | tf_op jit(solution)/shard_map/broadcast_in_dim | solution.py:13
  160.6 3.0 collective-permute-start.5
  165.0 52.7 %collective-permute-done.4 = bf16[256,3072]{0,1:T(8,128)(2,1)} collective-permute-done((bf16[256,3072]{0,1:T(8,128)(2,1)}, bf16[256,3072]{0,1:T(8,128)(2,1)}, u32[]{:S(2)}, u32[]{:S(2)}) %collective-permute-start.4) | collective-permute-done | bytes 1572896 | tf_op jit(solution)/shard_map/ppermute | solution.py:18
  217.7 2.5 collective-permute-start.6
  220.2 1.4 constant_dynamic-update-slice_fusion.5
  221.6 2.7 constant_dynamic-update-slice_fusion.4
  224.3 2.9 constant_dynamic-update-slice_fusion.3
  227.2 2.8 constant_dynamic-update-slice_fusion.2
  231.3 23.9 %collective-permute-done.6 = bf16[256,3072]{0,1:T(8,128)(2,1)S(1)} collective-permute-done((bf16[256,3072]{0,1:T(8,128)(2,1)}, bf16[256,3072]{0,1:T(8,128)(2,1)S(1)}, u32[]{:S(2)}, u32[]{:S(2)}) %collective-permute-start.6) | collective-permute-done | bytes 1572896 | tf_op jit(solution)/shard_map/ppermute | solution.py:18
  256.6 15.8 %fusion.2 = f32[1024,3072]{1,0:T(8,128)S(1)} fusion(bf16[2048,3072]{0,1:T(8,128)(2,1)} %constant_dynamic-update-slice_fusion, bf16[1024,2048]{1,0:T(8,128)(2,1)S(1)} %copy-done.1, f32[1024]{0:T(1024)S(1)} %add_rsqrt_fusion), kind=kOutput, calls=%fused_computation.5 | convolution fusion | flops 12891193344 | bytes 29364224 | tf_op jit(solution)/shard_map/dot_general | solution.py:58
  272.5 4.5 fusion.5
  277.0 4.5 fusion.6
  281.7 2.0 copy.22
  285.0 2.7 dynamic-slice_bitcast_fusion
  287.7 23.1 %all-gather.5.cloned.1.call-done = bf16[2,1024,768]{1,0,2:T(2,128)(2,1)} async-done(((bf16[2,1024,192]{1,0,2:T(2,128)(2,1)}), bf16[2,1024,768]{1,0,2:T(2,128)(2,1)}) %all-gather.5.cloned.1.call-update) | async-done | bytes 3145744 | tf_op jit(solution)/shard_map/all_gather | solution.py:66
  310.8 7.8 %fusion.7 = (bf16[1,1024,768]{1,0,2:T(2,128)(2,1)S(1)}, bf16[1,1024,768]{1,0,2:T(2,128)(2,1)S(1)}) fusion(bf16[2,1024,768]{1,0,2:T(2,128)(2,1)} %all-gather.5.cloned.1.call-done), kind=kLoop, calls=%fused_computation.55 | loop fusion | bytes 6291456 | tf_op jit(solution)/shard_map/slice | solution.py:76
  319.8 92.5 %all-gather.3.cloned.1.call-done = bf16[6144,512]{1,0:T(8,128)(2,1)} async-done(((bf16[768,512]{1,0:T(8,128)(2,1)}), bf16[6144,512]{1,0:T(8,128)(2,1)}) %all-gather.3.cloned.1.call-update) | async-done | bytes 6291472 | tf_op jit(solution)/shard_map/all_gather | solution.py:41
  413.5 2.4 copy.30
  416.4 7.3 %reduce.32 = bf16[768,512]{1,0:T(8,128)(2,1)} reduce(bf16[768,1,512]{2,1,0:T(2,128)(2,1)} %bitcast.36, bf16[]{:T(256)} %broadcast.133), dimensions={1}, to_apply=%bitcast.32.reduce_sub_computation | reduce | bytes 1572866
  423.7 2.4 reshape.117
  426.0 4.4 all-to-all-start
  430.5 1.9 select_select_fusion
  432.3 9.9 %convolution_convert_fusion = bf16[1024,512]{1,0:T(8,128)(2,1)} fusion(bf16[1024,6144]{0,1:T(8,128)(2,1)S(1)} %bitcast.33, bf16[6144,512]{1,0:T(8,128)(2,1)} %all-gather.3.cloned.1.call-done), kind=kOutput, calls=%fused_computation.10 | convolution fusion | flops 6442975232 | bytes 19922944 | tf_op jit(solution)/shard_map/dot_general | solution.py:78
  442.2 2.4 reshape.118
  (43 shorter events, 12.2 us)
Async XLA Ops:
  7.2 145.6 %copy-start.6 = (f32[1024,2]{0,1:T(2,128)S(1)}, f32[1024,2]{0,1:T(2,128)}, u32[]{:S(2)}) copy-start(f32[1024,2]{0,1:T(2,128)} %param.13) | copy-start | bytes 24580
  7.2 145.6 %copy-start.5 = (s32[1024,2]{0,1:T(2,128)S(1)}, s32[1024,2]{0,1:T(2,128)}, u32[]{:S(2)}) copy-start(s32[1024,2]{0,1:T(2,128)} %param.12) | copy-start | bytes 24580
  7.2 303.6 %all-gather.5.cloned.1.call-start = ((), (), s32[]{:S(2)}) async-start(), calls=%async_computation.2 | async-start | bytes 3932160 | tf_op jit(solution)/shard_map/all_gather | solution.py:66
  7.2 144.5 %copy-start = (bf16[1024,2048]{1,0:T(8,128)(2,1)S(1)}, bf16[1024,2048]{1,0:T(8,128)(2,1)}, u32[]{:S(2)}) copy-start(bf16[1024,2048]{1,0:T(8,128)(2,1)} %param.7) | copy-start | bytes 12582916
  9.8 70.4 %collective-permute-start = (bf16[256,3072]{0,1:T(8,128)(2,1)S(1)}, bf16[256,3072]{0,1:T(8,128)(2,1)S(1)}, u32[]{:S(2)}, u32[]{:S(2)}) collective-permute-start(bf16[256,3072]{0,1:T(8,128)(2,1)S(1)} %bitcast.38), channel_id=1, source_target_pairs={{0,4},{4,8},{8,12},{12,16},{16,20},{20,24},{24,28},{28,0},{1,5},{5... | collective-permute-start | bytes 4718600 | tf_op jit(solution)/shard_map/ppermute | solution.py:18
  12.8 69.8 %collective-permute-start.1 = (bf16[256,3072]{0,1:T(8,128)(2,1)S(1)}, bf16[256,3072]{0,1:T(8,128)(2,1)S(1)}, u32[]{:S(2)}, u32[]{:S(2)}) collective-permute-start(bf16[256,3072]{0,1:T(8,128)(2,1)S(1)} %bitcast.39), channel_id=1, source_target_pairs={{0,28},{4,0},{8,4},{12,8},{16,12},{20,16},{24,20},{28,24},{1,29},{... | collective-permute-start | bytes 4718600 | tf_op jit(solution)/shard_map/ppermute | solution.py:23
  80.2 2.5 copy-start.3
  80.2 69.0 %collective-permute-start.2 = (bf16[256,3072]{0,1:T(8,128)(2,1)S(1)}, bf16[256,3072]{0,1:T(8,128)(2,1)}, u32[]{:S(2)}, u32[]{:S(2)}) collective-permute-start(bf16[256,3072]{0,1:T(8,128)(2,1)S(1)} %collective-permute-done), channel_id=1, source_target_pairs={{0,4},{4,8},{8,12},{12,16},{16,20},{20,24},{24,28},{28,0},{1,5},{5... | collective-permute-start | bytes 4718600 | tf_op jit(solution)/shard_map/ppermute | solution.py:18
  82.6 77.9 %collective-permute-start.3 = (bf16[256,3072]{0,1:T(8,128)(2,1)S(1)}, bf16[256,3072]{0,1:T(8,128)(2,1)}, u32[]{:S(2)}, u32[]{:S(2)}) collective-permute-start(bf16[256,3072]{0,1:T(8,128)(2,1)S(1)} %collective-permute-done.1), channel_id=1, source_target_pairs={{0,28},{4,0},{8,4},{12,8},{16,12},{20,16},{24,20},{28,24},{1,29},{... | collective-permute-start | bytes 4718600 | tf_op jit(solution)/shard_map/ppermute | solution.py:23
  149.1 68.6 %collective-permute-start.4 = (bf16[256,3072]{0,1:T(8,128)(2,1)}, bf16[256,3072]{0,1:T(8,128)(2,1)}, u32[]{:S(2)}, u32[]{:S(2)}) collective-permute-start(bf16[256,3072]{0,1:T(8,128)(2,1)} %collective-permute-done.2), channel_id=1, source_target_pairs={{0,4},{4,8},{8,12},{12,16},{16,20},{20,24},{24,28},{28,0},{1,5},{5... | collective-permute-start | bytes 4718600 | tf_op jit(solution)/shard_map/ppermute | solution.py:18
  153.0 10.6 %copy-start.4 = (bf16[256,3072]{0,1:T(8,128)(2,1)S(1)}, bf16[256,3072]{0,1:T(8,128)(2,1)}, u32[]{:S(2)}) copy-start(bf16[256,3072]{0,1:T(8,128)(2,1)} %copy-done.3) | copy-start | bytes 4718596
  160.6 69.4 %collective-permute-start.5 = (bf16[256,3072]{0,1:T(8,128)(2,1)}, bf16[256,3072]{0,1:T(8,128)(2,1)S(1)}, u32[]{:S(2)}, u32[]{:S(2)}) collective-permute-start(bf16[256,3072]{0,1:T(8,128)(2,1)} %collective-permute-done.3), channel_id=1, source_target_pairs={{0,28},{4,0},{8,4},{12,8},{16,12},{20,16},{24,20},{28,24},{1,29},{... | collective-permute-start | bytes 4718600 | tf_op jit(solution)/shard_map/ppermute | solution.py:23
  217.7 37.6 %collective-permute-start.6 = (bf16[256,3072]{0,1:T(8,128)(2,1)}, bf16[256,3072]{0,1:T(8,128)(2,1)S(1)}, u32[]{:S(2)}, u32[]{:S(2)}) collective-permute-start(bf16[256,3072]{0,1:T(8,128)(2,1)} %collective-permute-done.4), channel_id=1, source_target_pairs={{0,4},{4,8},{8,12},{12,16},{16,20},{20,24},{24,28},{28,0},{1,5},{5... | collective-permute-start | bytes 4718600 | tf_op jit(solution)/shard_map/ppermute | solution.py:18
  224.3 32.3 %copy-start.1 = (bf16[1024,2048]{1,0:T(8,128)(2,1)S(1)}, bf16[1024,2048]{1,0:T(8,128)(2,1)}, u32[]{:S(2)}) copy-start(bf16[1024,2048]{1,0:T(8,128)(2,1)} %param.7) | copy-start | bytes 12582916
  277.0 7.0 %copy-start.2 = (f32[8,96,512]{2,1,0:T(8,128)S(1)}, f32[8,96,512]{2,1,0:T(8,128)}, u32[]{:S(2)}) copy-start(f32[8,96,512]{2,1,0:T(8,128)} %param.11) | copy-start | bytes 4718596
  283.8 128.5 %all-gather.3.cloned.1.call-start = ((), (), s32[]{:S(2)}) async-start(), calls=%async_computation.1 | async-start | bytes 7077888 | tf_op jit(solution)/shard_map/all_gather | solution.py:41
  426.0 16.2 %all-to-all-start = ((bf16[4,2,49152]{2,1,0:T(2,128)(2,1)}), bf16[4,2,49152]{2,1,0:T(2,128)(2,1)}, u32[]{:S(2)}, u32[]{:S(2)}) async-start(bf16[4,2,49152]{2,1,0:T(2,128)(2,1)} %reshape.117), calls=%async_computation | async-start | bytes 1572864 | tf_op jit(solution)/shard_map/all_to_all | solution.py:88
Sparse Core Ops, SparseCore 0:
  283.9 26.8 all-gather.4
  313.6 98.6 all-gather.2
